TPU v7x, 32 devices: a whole 2x2x4 slice. The times are simulated.
32 devices in a mesh: sp: 4 (over y, x), tp: 8 (over z, core).
Axes of the slice: x: 2, y: 2, z: 4, core: 2. Of those that a mesh axis runs over, the one named last changes fastest.
Arguments:
- tokens: bfloat16 [2048, 2048], P(('sp', 'tp')), may hold values from -6 to 6
- query_vectors: bfloat16 [2048, 2048], P('sp', 'tp'), may hold values from -8 to 8
- key_vectors: bfloat16 [2048, 2048], P('sp', 'tp'), may hold values from -8 to 8
- value_vectors: bfloat16 [2048, 2048], P('sp', 'tp'), may hold values from -24 to 24
- cum_gate: float32 [2048, 32], P('sp', 'tp'), may hold values from -260 to 0, as said below
- out_weight: bfloat16 [2048, 2048], P('tp'), may hold values from -0.125 to 0.125
- norm_gain: float32 [2048], replicated, may hold values from 0.1 to 1.9
- gate_weight: bfloat16 [4, 2048, 7168], P('sp', None, 'tp'), may hold values from -0.125 to 0.125
- up_weight: bfloat16 [4, 2048, 7168], P('sp', None, 'tp'), may hold values from -0.125 to 0.125
- down_weight: bfloat16 [4, 7168, 2048], P('sp', 'tp'), may hold values from -0.0625 to 0.0625
- expert_ids: int32 [2048, 2], P(('sp', 'tp')), may hold values from 0 to 3, all different within a row; in each aligned block of 64 rows (0 to 63, 64 to 127, ...) at most 48 rows name the same one
- route_weights: float32 [2048, 2], P(('sp', 'tp')), may hold values from 0.2 to 1
Outputs:
- layer_output: bfloat16 [2048, 2048], P(('sp', 'tp'))
Inputs may be any that keep to these rules, and one draw needn't show every extreme that they name: `cum_gate`: along the positions each head's values never rise. `expert_ids`: within the rows of one device no expert is named by more than 48 rows, and in some devices' rows one expert is named by exactly 48; a row names 2 different experts.
All inputs are finite; a program needn't handle non-finite values.
Results may differ from a plain program's by a relative error of at most 0.014.
Values may be sent and summed in bfloat16 or wider, within the bound.
A program may use at most 128 MiB of HBM per device.

v0:
```python
import math

import jax
import jax.numpy as jnp
from jax import lax
from jax.sharding import PartitionSpec as P

NEG_LARGE = -1e30


def shards(
    tokens,
    query_vectors,
    key_vectors,
    value_vectors,
    cum_gate,
    out_weight,
    norm_gain,
    gate_weight,
    up_weight,
    down_weight,
    expert_ids,
    route_weights,
):
    sp_count = lax.axis_size("sp")
    seg_rows = query_vectors.shape[0]
    heads_here = cum_gate.shape[1]
    head_width = query_vectors.shape[1] // heads_here
    score_scale = head_width ** (-0.5)
    offset = lax.axis_index("sp") * seg_rows
    last_query = offset + seg_rows - 1
    query_pos = offset + jnp.arange(seg_rows, dtype=jnp.int32)
    query_heads = query_vectors.reshape(seg_rows, heads_here, head_width)
    query_gate = cum_gate.T
    gate_rows = lax.all_gather(cum_gate, "sp", axis=0, tiled=True)

    def attend_block(carried, key_block, value_block, block_start):
        running_peak, running_total, accumulated = carried
        row_count = key_block.shape[0]
        key_heads = key_block.reshape(row_count, heads_here, head_width)
        value_heads = value_block.reshape(row_count, heads_here, head_width)
        key_gate = lax.dynamic_slice_in_dim(gate_rows, block_start, row_count, 0).T
        scores = (
            jnp.einsum("qhd,khd->hqk", query_heads, key_heads, preferred_element_type=jnp.float32)
            * score_scale
        )
        scores = scores + query_gate[:, :, None] - key_gate[:, None, :]
        key_pos = block_start + jnp.arange(row_count, dtype=jnp.int32)
        visible = (key_pos[None, :] <= query_pos[:, None])[None]
        scores = jnp.where(visible, scores, NEG_LARGE)
        new_peak = jnp.maximum(running_peak, jnp.max(scores, axis=2))
        exponent = jnp.where(visible, jnp.exp(scores - new_peak[:, :, None]), 0.0)
        rescale = jnp.exp(running_peak - new_peak)
        running_total = running_total * rescale + jnp.sum(exponent, axis=2)
        weighted = jnp.einsum(
            "hqk,khd->hqd",
            exponent.astype(jnp.bfloat16),
            value_heads,
            preferred_element_type=jnp.float32,
        )
        accumulated = accumulated * rescale[:, :, None] + weighted
        return (new_peak, running_total, accumulated)

    start_state = (
        jnp.full((heads_here, seg_rows), NEG_LARGE, jnp.float32),
        jnp.zeros((heads_here, seg_rows), jnp.float32),
        jnp.zeros((heads_here, seg_rows, head_width), jnp.float32),
    )
    carried = start_state
    key_piece = lax.all_gather(key_vectors, "sp", axis=0, tiled=True)
    value_piece = lax.all_gather(value_vectors, "sp", axis=0, tiled=True)
    row_count = key_piece.shape[0]
    block_rows = math.gcd(row_count, 1024)
    block_count = row_count // block_rows
    key_stack = key_piece.reshape(block_count, block_rows, key_piece.shape[1])
    value_stack = value_piece.reshape(block_count, block_rows, value_piece.shape[1])

    def step_block(state, inputs):
        key_block, value_block, block_index = inputs
        block_start = block_index * block_rows

        def take_block(inner):
            return attend_block(inner, key_block, value_block, block_start)

        def skip_block(inner):
            return inner

        return (lax.cond(block_start <= last_query, take_block, skip_block, state), None)

    carried, _ = lax.scan(
        step_block, carried, (key_stack, value_stack, jnp.arange(block_count, dtype=jnp.int32))
    )
    final_peak, final_total, accumulated = carried
    attended = (accumulated / final_total[:, :, None]).astype(jnp.bfloat16)
    attended = attended.transpose(1, 0, 2).reshape(seg_rows, heads_here * head_width)
    tok_dev = tokens.shape[0]
    model_width = tokens.shape[1]
    token_rows = lax.all_to_all(attended, "tp", split_axis=0, concat_axis=1, tiled=True)
    projected = jnp.dot(
        token_rows,
        lax.all_gather(out_weight, "tp", axis=0, tiled=True),
        preferred_element_type=jnp.float32,
    )
    stream_wide = (tokens.astype(jnp.float32) + projected).astype(jnp.bfloat16).astype(jnp.float32)
    inverse = lax.rsqrt(jnp.mean(stream_wide * stream_wide, axis=1, keepdims=True) + 1e-05)
    normed = (stream_wide * inverse * norm_gain[None, :]).astype(jnp.bfloat16)
    n_experts = gate_weight.shape[0] * sp_count
    top_count = expert_ids.shape[1]
    capacity = max(2, 3 * tok_dev * top_count // (2 * n_experts))
    flat_ids = expert_ids.reshape(-1)
    hits = (flat_ids[:, None] == jnp.arange(n_experts, dtype=jnp.int32)[None, :]).astype(jnp.int32)
    earlier = jnp.cumsum(hits, axis=0) - hits
    slot_index = flat_ids * capacity + jnp.sum(earlier * hits, axis=1)
    placement_map = (
        jnp.arange(n_experts * capacity, dtype=jnp.int32)[:, None] == slot_index[None, :]
    ).astype(jnp.bfloat16)
    repeated = jnp.repeat(normed, top_count, axis=0)
    dispatch = jnp.dot(placement_map, repeated, preferred_element_type=jnp.float32).astype(
        jnp.bfloat16
    )
    dispatch = dispatch.reshape(n_experts, capacity, model_width)
    arrived = lax.all_to_all(dispatch, "sp", split_axis=0, concat_axis=0, tiled=True)
    row_block = arrived.reshape(-1, model_width)
    rows_in = lax.all_gather(row_block, "tp", axis=0, tiled=True)
    gate_value = jnp.dot(rows_in, gate_weight[0], preferred_element_type=jnp.float32)
    up_value = jnp.dot(rows_in, up_weight[0], preferred_element_type=jnp.float32)
    hidden = (jax.nn.silu(gate_value) * up_value).astype(jnp.bfloat16)
    summed = lax.psum_scatter(
        jnp.dot(hidden, down_weight[0], preferred_element_type=jnp.float32).astype(jnp.bfloat16),
        "tp",
        scatter_dimension=0,
        tiled=True,
    )
    returned = summed.reshape(arrived.shape)
    back = lax.all_to_all(returned, "sp", split_axis=0, concat_axis=0, tiled=True)
    flat_back = back.reshape(n_experts * capacity, model_width)
    picked = flat_back[slot_index].astype(jnp.float32).reshape(tok_dev, top_count, model_width)
    mixture = jnp.sum(picked * route_weights[:, :, None], axis=1)
    return (stream_wide + mixture).astype(jnp.bfloat16)


def solution(mesh):
    in_specs = (
        P(("sp", "tp"), None),
        P("sp", "tp"),
        P("sp", "tp"),
        P("sp", "tp"),
        P("sp", "tp"),
        P("tp", None),
        P(),
        P("sp", None, "tp"),
        P("sp", None, "tp"),
        P("sp", "tp", None),
        P(("sp", "tp"), None),
        P(("sp", "tp"), None),
    )
    out_specs = P(("sp", "tp"), None)
    return jax.shard_map(shards, mesh=mesh, in_specs=in_specs, out_specs=out_specs, check_vma=False)
```

profile of v0, /device:TPU:0, one launch (start us, length us, event | category | flops | bytes accessed | tf_op | source)
XLA Modules:
  0.0 362.4 jit_solution(4247297287543457111)
XLA Ops:
  6.5 0.7 all-gather.5.cloned.1.call-update
  7.3 0.7 all-gather.7.cloned.1.call-update
  8.1 0.7 all-gather.9.cloned.1.call-update
  8.7 1.1 copy.27
  9.8 0.8 copy.32
  10.8 9.8 %all_gather.16 = f32[2048,4]{0,1:T(4,128)S(1)} all-gather(f32[512,4]{0,1:T(4,128)} %param.20), channel_id=1, replica_groups=mesh['sp'=4,'tp'=8] {'sp'}, dimensions={0}, use_global_device_ids=true | all-gather | bytes 40960 | tf_op jit(solution)/shard_map/all_gather | solution.py:35
  20.6 17.9 %all-gather.5.cloned.1.call-done = bf16[2048,256]{1,0:T(8,128)(2,1)} async-done(((bf16[512,256]{1,0:T(8,128)(2,1)}), bf16[2048,256]{1,0:T(8,128)(2,1)}) %all-gather.5.cloned.1.call-update) | async-done | bytes 1048592 | tf_op jit(solution)/shard_map/all_gather | solution.py:70
  38.4 1.5 copy.28
  39.9 26.9 %all-gather.7.cloned.1.call-done = bf16[2048,256]{1,0:T(8,128)(2,1)} async-done(((bf16[512,256]{1,0:T(8,128)(2,1)}), bf16[2048,256]{1,0:T(8,128)(2,1)}) %all-gather.7.cloned.1.call-update) | async-done | bytes 1048592 | tf_op jit(solution)/shard_map/all_gather | solution.py:71
  66.8 1.5 copy.29
  68.4 12.0 %while.15 = (s32[]{:T(128)}, f32[4,512]{1,0:T(4,128)S(1)}, f32[4,512]{1,0:T(4,128)S(1)}, f32[4,512,64]{1,2,0:T(8,128)S(1)}, s32[2]{0:T(128)S(1)}, /*index=5*/s32...) while((s32[]{:T(128)}, f32[4,512]{1,0:T(4,128)S(1)}, ...), condition=%wide.region_5.6_spmd.clone, body=%wide.region_0.5_spmd.clone.sunk | while | flops 577508864 | bytes 31973748 | solution.py:90
  68.4 0.7 dynamic_slice.31
  69.8 9.2 %conditional.3 = ((f32[4,512]{1,0:T(4,128)S(1)}, f32[4,512]{1,0:T(4,128)S(1)}, f32[4,512,64]{1,2,0:T(8,128)S(1)})) conditional(s32[]{:T(128)} %convert_element_type.83, (f32[4,512]{1,0:T(4,128)S(1)}, f32[4,512]{1,0:T(4,128)S(1)}, f32[4,512,64]{1,2,0:T(8,128)S(1)}) %tuple.42, (s32[]{:T(128)}, s32[]{:T(128)}, bf16[2,1024,256]{1,2,0:T(8,128)(2,1)S(1)}, ...), branch_computations={%region_1.1_spmd, %region_2.4_spmd} | conditional | flops 577508864 | bytes 31971410 | solution.py:88
  70.4 2.5 fusion.4
  72.9 2.9 fusion.3
  75.8 3.2 fusion.8
  79.0 0.7 dynamic_slice.31
  80.8 1.0 copy.30
  81.8 4.6 %all-to-all-start = ((bf16[8,64,256]{2,1,0:T(8,128)(2,1)}), bf16[8,64,256]{2,1,0:T(8,128)(2,1)S(1)}, u32[]{:S(2)}, u32[]{:S(2)}) async-start(bf16[8,64,256]{2,1,0:T(8,128)(2,1)} %copy.30), calls=%async_computation | async-start | bytes 524288 | tf_op jit(solution)/shard_map/all_to_all | solution.py:98
  86.9 15.4 %all-to-all-done = bf16[8,64,256]{2,1,0:T(8,128)(2,1)S(1)} async-done(((bf16[8,64,256]{2,1,0:T(8,128)(2,1)}), bf16[8,64,256]{2,1,0:T(8,128)(2,1)S(1)}, u32[]{:S(2)}, u32[]{:S(2)}) %all-to-all-start) | async-done | bytes 262176 | tf_op jit(solution)/shard_map/all_to_all | solution.py:98
  102.3 53.7 %all-gather.9.cloned.1.call-done = bf16[2048,2048]{1,0:T(8,128)(2,1)} async-done(((bf16[256,2048]{1,0:T(8,128)(2,1)}), bf16[2048,2048]{1,0:T(8,128)(2,1)}) %all-gather.9.cloned.1.call-update) | async-done | bytes 8388624 | tf_op jit(solution)/shard_map/all_gather | solution.py:101
  156.0 5.1 %multiply_reduce_fusion.1 = (f32[64]{0:T(128)S(1)}, f32[64,2048]{1,0:T(8,128)S(1)}) fusion(bf16[64,2048]{1,0:T(8,128)(2,1)S(1)} %bitcast.63, bf16[2048,2048]{1,0:T(8,128)(2,1)} %all-gather.9.cloned.1.call-done, bf16[64,2048]{1,0:T(8,128)(2,1)S(1)} %copy-done.1), kind=kOutput, calls=%fused_computation.35 | convolution fusion | flops 537657280 | bytes 9437440 | tf_op jit(solution)/shard_map/dot_general | solution.py:99
  162.1 15.3 %all_to_all.29 = bf16[4,48,2048]{2,1,0:T(8,128)(2,1)} all-to-all(bf16[4,48,2048]{2,1,0:T(8,128)(2,1)S(1)} %bitcast.62), channel_id=1, replica_groups=mesh['sp'=4,'tp'=8] {'sp'}, dimensions={0} | all-to-all | bytes 1572864 | tf_op jit(solution)/shard_map/all_to_all | solution.py:122
  177.5 61.7 %all-gather.11.cloned.1.call-done = bf16[1536,2048]{1,0:T(8,128)(2,1)} async-done(((bf16[192,2048]{1,0:T(8,128)(2,1)}), bf16[1536,2048]{1,0:T(8,128)(2,1)}) %all-gather.11.cloned.1.call-update) | async-done | bytes 6291472 | tf_op jit(solution)/shard_map/all_gather | solution.py:124
  239.3 11.4 %fusion.18 = f32[1536,896]{1,0:T(8,128)} fusion(bf16[1536,2048]{1,0:T(8,128)(2,1)} %all-gather.11.cloned.1.call-done, bf16[1,2048,896]{2,1,0:T(8,128)(2,1)} %param.23), kind=kOutput, calls=%fused_computation.25 | convolution fusion | flops 5637144576 | bytes 15466496 | tf_op jit(solution)/shard_map/dot_general | solution.py:125
  250.6 20.1 %convolution_convert_fusion = bf16[1536,2048]{1,0:T(8,128)(2,1)} fusion(bf16[1,896,2048]{2,1,0:T(8,128)(2,1)} %param.25, f32[1536,896]{1,0:T(8,128)} %fusion.18, bf16[1536,2048]{1,0:T(8,128)(2,1)} %all-gather.11.cloned.1.call-done, bf16[1,2048,896]{2,1,0:T(8,128)(2,1)} %param.24), kind=kOutput, calls=%fused_computation.21 | convolution fusion | flops 11285692416 | bytes 25427968 | tf_op jit(solution)/shard_map/dot_general | solution.py:129
  270.7 68.5 %reduce-scatter.2.cloned.1.call-done = bf16[192,2048]{1,0:T(8,128)(2,1)} async-done(((bf16[1536,2048]{1,0:T(8,128)(2,1)}), bf16[192,2048]{1,0:T(8,128)(2,1)}) %reduce-scatter.2.cloned.1.call-update) | async-done | bytes 786448 | tf_op jit(solution)/shard_map/reduce_scatter | solution.py:128
  339.2 3.7 %all-to-all-start.2 = ((bf16[4,48,2048]{2,1,0:T(8,128)(2,1)}), bf16[4,48,2048]{2,1,0:T(8,128)(2,1)S(1)}, u32[]{:S(2)}, u32[]{:S(2)}) async-start(bf16[4,48,2048]{2,1,0:T(8,128)(2,1)} %bitcast.67), calls=%async_computation.3 | async-start | bytes 1572864 | tf_op jit(solution)/shard_map/all_to_all | solution.py:135
  343.3 8.7 %all-to-all-done.2 = bf16[4,48,2048]{2,1,0:T(8,128)(2,1)S(1)} async-done(((bf16[4,48,2048]{2,1,0:T(8,128)(2,1)}), bf16[4,48,2048]{2,1,0:T(8,128)(2,1)S(1)}, u32[]{:S(2)}, u32[]{:S(2)}) %all-to-all-start.2) | async-done | bytes 786464 | tf_op jit(solution)/shard_map/all_to_all | solution.py:135
  352.0 0.9 gather_fusion
  353.6 1.5 multiply_reduce_fusion
  355.1 0.8 add_convert_fusion
  (52 shorter events, 3.7 us)
Async XLA Ops:
  6.5 61.8 %copy-start = (f32[512,4]{0,1:T(4,128)S(1)}, f32[512,4]{0,1:T(4,128)}, u32[]{:S(2)}) copy-start(f32[512,4]{0,1:T(4,128)} %param.20) | copy-start | bytes 24580
  6.5 31.9 %all-gather.5.cloned.1.call-start = ((), (), s32[]{:S(2)}) async-start(), calls=%async_computation.4 | async-start | bytes 1310720 | tf_op jit(solution)/shard_map/all_gather | solution.py:70
  7.3 59.5 %all-gather.7.cloned.1.call-start = ((), (), s32[]{:S(2)}) async-start(), calls=%async_computation.5 | async-start | bytes 1310720 | tf_op jit(solution)/shard_map/all_gather | solution.py:71
  8.0 148.0 %all-gather.9.cloned.1.call-start = ((), (), s32[]{:S(2)}) async-start(), calls=%async_computation.6 | async-start | bytes 9437184 | tf_op jit(solution)/shard_map/all_gather | solution.py:101
  68.4 87.6 %copy-start.1 = (bf16[64,2048]{1,0:T(8,128)(2,1)S(1)}, bf16[64,2048]{1,0:T(8,128)(2,1)}, u32[]{:S(2)}) copy-start(bf16[64,2048]{1,0:T(8,128)(2,1)} %param.16) | copy-start | bytes 786436
  81.8 20.5 %all-to-all-start = ((bf16[8,64,256]{2,1,0:T(8,128)(2,1)}), bf16[8,64,256]{2,1,0:T(8,128)(2,1)S(1)}, u32[]{:S(2)}, u32[]{:S(2)}) async-start(bf16[8,64,256]{2,1,0:T(8,128)(2,1)} %copy.30), calls=%async_computation | async-start | bytes 524288 | tf_op jit(solution)/shard_map/all_to_all | solution.py:98
  86.4 152.9 %all-gather.11.cloned.1.call-start = ((), (), s32[]{:S(2)}) async-start(), calls=%async_computation.7 | async-start | bytes 7077888 | tf_op jit(solution)/shard_map/all_gather | solution.py:124
  156.0 5.1 %copy-start.2 = (f32[2048]{0:T(1024)S(1)}, f32[2048]{0:T(1024)}, u32[]{:S(2)}) copy-start(f32[2048]{0:T(1024)} %param.22) | copy-start | bytes 24580
  177.5 161.8 %reduce-scatter.2.cloned.1.call-start = ((), (), s32[]{:S(2)}) async-start(), calls=%async_computation.8 | async-start | bytes 7077888 | tf_op jit(solution)/shard_map/reduce_scatter | solution.py:128
  270.7 72.2 %copy-start.3 = (s32[64,2]{0,1:T(2,128)S(1)}, s32[64,2]{0,1:T(2,128)}, u32[]{:S(2)}) copy-start(s32[64,2]{0,1:T(2,128)} %param.26) | copy-start | bytes 1540
  270.7 72.5 %copy-start.4 = (f32[64,2]{0,1:T(2,128)S(1)}, f32[64,2]{0,1:T(2,128)}, u32[]{:S(2)}) copy-start(f32[64,2]{0,1:T(2,128)} %param.27) | copy-start | bytes 1540
  339.2 12.8 %all-to-all-start.2 = ((bf16[4,48,2048]{2,1,0:T(8,128)(2,1)}), bf16[4,48,2048]{2,1,0:T(8,128)(2,1)S(1)}, u32[]{:S(2)}, u32[]{:S(2)}) async-start(bf16[4,48,2048]{2,1,0:T(8,128)(2,1)} %bitcast.67), calls=%async_computation.3 | async-start | bytes 1572864 | tf_op jit(solution)/shard_map/all_to_all | solution.py:135
Sparse Core Ops, SparseCore 0:
  9.2 29.2 all-gather.4
  40.3 26.4 all-gather.6
  68.4 87.5 all-gather.8
  177.6 61.6 all-gather.10
  270.8 68.3 reduce-scatter.1
where the time goes:
time: 363 us; the launch traced here: 362 us
  waiting for transfers between devices  255 us (70%)
  matrix products  42.6 us (12%)
  blocking collectives  25.1 us (7%)
  between operations  13.4 us (4%)
  local copies, waits for them, and re-layouts  10.3 us (3%)
  starting transfers between devices  8.43 us (2%)
  other arithmetic  6.2 us (2%)
    reduce_scatter x1, waiting for transfers between devices, shards(): lax.psum_scatter(jnp.dot(hidden, down_weight[0], preferred_element_type=j...  68.5 us
    all_gather x1, waiting for transfers between devices, shards(): rows_in = lax.all_gather(row_block, 'tp', axis=0, tiled=True)  61.7 us
    all_gather x1, waiting for transfers between devices, shards(): lax.all_gather(out_weight, 'tp', axis=0, tiled=True)  53.7 us
    all_gather x1, waiting for transfers between devices, shards(): value_piece = lax.all_gather(value_vectors, 'sp', axis=0, tiled=True)  26.9 us
    dot_general x1, matrix products, shards(): jnp.dot(hidden, down_weight[0], preferred_element_type=jnp.float32)  20.1 us
    all_gather x1, waiting for transfers between devices, shards(): key_piece = lax.all_gather(key_vectors, 'sp', axis=0, tiled=True)  17.9 us
    all_to_all x1, waiting for transfers between devices, shards(): lax.all_to_all(attended, 'tp', split_axis=0, concat_axis=1, tiled=True)  15.4 us
    all_to_all x1, blocking collectives, shards(): lax.all_to_all(dispatch, 'sp', split_axis=0, concat_axis=0, tiled=True)  15.3 us
  transfers between devices with their start and end apart: 7, of which 7 were waited for; matrix products, arithmetic and copies ran while one was open for 5% of the time, Pallas kernels for 0%

commit v1 on v0

v1 whole, which is shorter than its diff:
```python
import functools
import math

import jax
import jax.numpy as jnp
from jax import lax
from jax.experimental import pallas as pl
from jax.experimental.pallas import tpu as pltpu
from jax.sharding import PartitionSpec as P

MESH = pl.DeviceIdType.MESH
VMEM_LIMIT = 60 * 1024 * 1024
F32 = jnp.float32
BF16 = jnp.bfloat16


def rcopy(src, dst, ssem, rsem, where):
    return pltpu.make_async_remote_copy(
        src_ref=src, dst_ref=dst, send_sem=ssem, recv_sem=rsem, device_id=where, device_id_type=MESH
    )


def vmem_specs(count):
    return [pl.BlockSpec(memory_space=pltpu.VMEM)] * count


def exchange_kernel(sp, k, v, g, ka, va, ga, ssem, rsem):
    s = lax.axis_index("sp")
    barrier = pltpu.get_barrier_semaphore()
    for d in range(1, sp):
        pl.semaphore_signal(barrier, inc=1, device_id={"sp": lax.rem(s + d, sp)}, device_id_type=MESH)
    pl.semaphore_wait(barrier, sp - 1)
    pairs = ((k, ka), (v, va), (g, ga))

    def copy(n, d, slot, target):
        src, dst = pairs[n]
        return rcopy(src, dst.at[slot], ssem.at[n, d], rsem.at[n, d], {"sp": target})

    for d in range(1, sp):

        @pl.when(s + d < sp)
        def _():
            for n in range(3):
                copy(n, d, s, s + d).start()

    for src, dst in pairs:
        dst[s] = src[...]
    for d in range(1, sp):

        @pl.when(s - d >= 0)
        def _():
            for n in range(3):
                copy(n, d, s - d, lax.rem(s + d, sp)).wait_recv()

    for d in range(1, sp):

        @pl.when(s + d < sp)
        def _():
            for n in range(3):
                copy(n, d, s, s + d).wait_send()


def attend_kernel(heads, q, ka, va, ga, w, out, att):
    s = lax.axis_index("sp")
    rows, width = q.shape
    hd = width // heads
    tile = math.gcd(rows, 256)
    log2e = 1.4426950408889634
    coef = hd ** (-0.5) * log2e
    for h in range(heads):
        cols = slice(h * hd, (h + 1) * hd)
        for i in range(rows // tile):
            qt = q[i * tile : (i + 1) * tile, cols]
            seen = (i + 1) * tile

            def scores(kb, gb):
                return (
                    lax.dot_general(qt, kb, (((1,), (1,)), ((), ())), preferred_element_type=F32) * coef
                    - gb * log2e
                )

            sc = scores(ka[s, 0:seen, cols], ga[s, h : h + 1, 0:seen])
            row = lax.broadcasted_iota(jnp.int32, sc.shape, 0) + i * tile
            col = lax.broadcasted_iota(jnp.int32, sc.shape, 1)
            sc = jnp.where(col <= row, sc, -1e30)
            peak = jnp.max(sc, axis=1, keepdims=True)
            ex = jnp.exp2(sc - peak)
            total = jnp.sum(ex, axis=1, keepdims=True)
            acc = jnp.dot(ex.astype(BF16), va[s, 0:seen, cols], preferred_element_type=F32)

            def step(b, carry):
                peak, total, acc = carry
                sc = scores(ka[b, :, cols], ga[b, h : h + 1, :])
                new = jnp.maximum(peak, jnp.max(sc, axis=1, keepdims=True))
                ex = jnp.exp2(sc - new)
                fix = jnp.exp2(peak - new)
                total = total * fix + jnp.sum(ex, axis=1, keepdims=True)
                acc = acc * fix + jnp.dot(ex.astype(BF16), va[b, :, cols], preferred_element_type=F32)
                return new, total, acc

            peak, total, acc = lax.fori_loop(0, s, step, (peak, total, acc))
            att[i * tile : (i + 1) * tile, cols] = (acc / total).astype(BF16)
    wide = w.shape[1]
    chunk = math.gcd(wide, 512)
    for n in range(wide // chunk):
        cut = slice(n * chunk, (n + 1) * chunk)
        out[:, cut] = jnp.dot(att[...], w[:, cut], preferred_element_type=F32).astype(BF16)


def greet(sp, zn, s, z, c, partner):
    barrier = pltpu.get_barrier_semaphore()
    pl.semaphore_signal(barrier, inc=1, device_id={"tp": partner}, device_id_type=MESH)
    for i in range(1, zn):
        pl.semaphore_signal(
            barrier, inc=1, device_id={"tp": 2 * lax.rem(z + i, zn) + c}, device_id_type=MESH
        )
    for d in range(1, sp):
        pl.semaphore_signal(barrier, inc=1, device_id={"sp": lax.rem(s + d, sp)}, device_id_type=MESH)
    pl.semaphore_wait(barrier, 1 + (zn - 1) + (sp - 1))


def dispatch_kernel(
    sp, zn, p, tok, gain, place, comb, stream, rows, combs,
    xr, cb, zr, ng, pg, db, xs, xrs, as_, ars, zs, zrs, ns, nrs, ds_, drs, fs, frs,
):
    s, t = lax.axis_index("sp"), lax.axis_index("tp")
    z, c = t // 2, lax.rem(t, 2)
    partner = t + 1 - 2 * c
    T = tok.shape[0]
    cap = rows.shape[3]
    greet(sp, zn, s, z, c, partner)

    def at_z(i):
        return 2 * lax.rem(z + i, zn) + c

    def swap(i):
        zz = lax.rem(z + 1 + i, zn)
        src = p.at[pl.ds(pl.multiple_of((2 * zz + 1 - c) * T, 16), T)]
        return rcopy(src, xr.at[i], xs.at[i], xrs.at[i], {"tp": partner})

    def aux(n, i):
        src, dst = ((place, pg), (comb, combs))[n]
        return rcopy(src, dst.at[i], as_.at[n, i], ars.at[n, i], {"tp": at_z(i)})

    def reduce_to(i):
        return rcopy(cb.at[i], zr.at[i], zs.at[i], zrs.at[i], {"tp": at_z(1 + i)})

    def spread(i):
        return rcopy(ng.at[0], ng.at[i], ns.at[i], nrs.at[i], {"tp": at_z(i)})

    def route(i, d):
        e = lax.rem(s + d, sp)
        return rcopy(db.at[i, e], rows.at[s, c, i], ds_.at[i, d], drs.at[i, d], {"sp": e})

    def routed_slot(i, d):
        return rows.at[lax.rem(s + sp - d, sp), c, i]

    def forward(i, d):
        ref = routed_slot(i, d)
        return rcopy(ref, ref, fs.at[i, d], frs.at[i, d], {"tp": partner})

    for i in range(zn):
        swap(i).start()
    for i in range(1, zn):
        for n in range(2):
            aux(n, i).start()
    pg[0] = place[...]
    combs[0] = comb[...]
    own = None
    for i in range(zn):
        swap(i).wait_recv()
        zz = lax.rem(z + 1 + i, zn)
        both = p[pl.ds(pl.multiple_of((2 * zz + c) * T, 16), T), :].astype(F32) + xr[i].astype(F32)
        if i < zn - 1:
            cb[i] = both.astype(BF16)
            reduce_to(i).start()
        else:
            own = both
    for i in range(zn - 1):
        reduce_to(i).wait_recv()
        own = own + zr[i].astype(F32)
    st = (tok[...].astype(F32) + own).astype(BF16)
    stream[...] = st
    wide = st.astype(F32)
    inverse = lax.rsqrt(jnp.mean(wide * wide, axis=1, keepdims=True) + 1e-05)
    ng[0] = (wide * inverse * gain[...]).astype(BF16)
    for i in range(1, zn):
        spread(i).start()
    for i in range(zn):
        if i > 0:
            aux(0, i).wait_recv()
            spread(i).wait_recv()
        moved = jnp.dot(pg[i], ng[i], preferred_element_type=F32).astype(BF16)
        for e in range(sp):
            db[i, e] = moved[e * cap : (e + 1) * cap]
        for d in range(1, sp):
            route(i, d).start()
        rows[s, c, i] = db[i, s]
        forward(i, 0).start()
    for i in range(zn):

        def arrive(d, _):
            rcopy(
                db.at[i, 0], routed_slot(i, d), ds_.at[i, d], drs.at[i, d], {"sp": lax.rem(s + d, sp)}
            ).wait_recv()
            forward(i, d).start()
            return 0

        lax.fori_loop(1, sp, arrive, 0)
    for i in range(zn):

        def landed(d, _):
            ref = rows.at[lax.rem(s + sp - d, sp), 1 - c, i]
            rcopy(ref, ref, fs.at[i, d], frs.at[i, d], {"tp": partner}).wait_recv()
            forward(i, d).wait_send()
            return 0

        lax.fori_loop(0, sp, landed, 0)
        swap(i).wait_send()
        if i < zn - 1:
            reduce_to(i).wait_send()
        if i > 0:
            spread(i).wait_send()
            aux(1, i).wait_recv()
            for n in range(2):
                aux(n, i).wait_send()
        for d in range(1, sp):
            route(i, d).wait_send()


def combine_kernel(
    sp, zn, y, combs, stream, out, pr, cs, eb, mb, rr, ps, prs, es, ers, ms, mrs
):
    s, t = lax.axis_index("sp"), lax.axis_index("tp")
    z, c = t // 2, lax.rem(t, 2)
    partner = t + 1 - 2 * c
    T = stream.shape[0]
    cap, wide = y.shape[3], y.shape[4]
    greet(sp, zn, s, z, c, partner)
    order = list(range(1, zn)) + [0]

    def peer(d):
        return lax.rem(s + d, sp)

    def swap(i, d):
        return rcopy(y.at[peer(d), 1 - c, i], pr.at[i, d], ps.at[i, d], prs.at[i, d], {"tp": partner})

    def back(i, d, slot):
        return rcopy(cs.at[i, d], eb.at[i, slot], es.at[i, d], ers.at[i, d], {"sp": peer(d)})

    def reduce_to(i):
        return rcopy(
            mb.at[i], rr.at[i], ms.at[i], mrs.at[i], {"tp": 2 * lax.rem(z + zn - i, zn) + c}
        )

    for i in order:
        for d in list(range(1, sp)) + [0]:
            swap(i, d).start()
    for i in order:

        def both(d):
            swap(i, d).wait_recv()
            return (y[peer(d), c, i].astype(F32) + pr[i, d].astype(F32)).astype(BF16)

        def send(d, _):
            cs[i, d] = both(d)
            back(i, d, s).start()
            return 0

        lax.fori_loop(1, sp, send, 0)
        eb[i, s] = both(0)
    own = None
    for i in order:
        for d in range(1, sp):
            back(i, d, lax.rem(s + sp - d, sp)).wait_recv()
        parts = eb[i].reshape(sp * cap, wide)
        mixed = jnp.dot(combs[i], parts, preferred_element_type=F32)
        mixed = mixed[0:T] + mixed[T : 2 * T]
        if i > 0:
            mb[i] = mixed.astype(BF16)
            reduce_to(i).start()
        else:
            own = mixed
    for i in range(1, zn):
        reduce_to(i).wait_recv()
        own = own + rr[i].astype(F32)
    out[...] = (stream[...].astype(F32) + own).astype(BF16)
    for i in range(zn):
        for d in range(sp):
            swap(i, d).wait_send()
            if d > 0:
                back(i, d, s).wait_send()
        if i > 0:
            reduce_to(i).wait_send()


def params(cid=None):
    if cid is None:
        return pltpu.CompilerParams(vmem_limit_bytes=VMEM_LIMIT)
    return pltpu.CompilerParams(
        collective_id=cid, has_side_effects=True, vmem_limit_bytes=VMEM_LIMIT
    )


def shards(
    tokens,
    query_vectors,
    key_vectors,
    value_vectors,
    cum_gate,
    out_weight,
    norm_gain,
    gate_weight,
    up_weight,
    down_weight,
    expert_ids,
    route_weights,
):
    sp = lax.axis_size("sp")
    tp = lax.axis_size("tp")
    zn = tp // 2
    seg, width = query_vectors.shape
    heads = cum_gate.shape[1]
    T, D = tokens.shape
    dma = pltpu.SemaphoreType.DMA

    n_experts = gate_weight.shape[0] * sp
    top = expert_ids.shape[1]
    cap = max(2, 3 * T * top // (2 * n_experts))
    cap = -(-cap // 16) * 16
    slots = n_experts * cap
    flat = expert_ids.reshape(-1)
    hits = (flat[:, None] == jnp.arange(n_experts, dtype=jnp.int32)[None, :]).astype(F32)
    lower = jnp.tril(jnp.ones((flat.shape[0], flat.shape[0]), F32), -1)
    earlier = jnp.dot(lower, hits, preferred_element_type=F32)
    slot = (flat * cap + jnp.sum(earlier * hits, axis=1).astype(jnp.int32)).reshape(T, top)
    match = slot[:, :, None] == jnp.arange(slots, dtype=jnp.int32)[None, None, :]
    place = jnp.any(match, axis=1).astype(BF16).T
    weight = jnp.sum(jnp.where(match, route_weights[:, :, None], 0.0), axis=1)
    high = lax.reduce_precision(weight, 8, 7)
    comb = jnp.concatenate([high, weight - high], axis=0).astype(BF16)

    kall, vall, gall = pl.pallas_call(
        functools.partial(exchange_kernel, sp),
        out_shape=(
            jax.ShapeDtypeStruct((sp, seg, width), BF16),
            jax.ShapeDtypeStruct((sp, seg, width), BF16),
            jax.ShapeDtypeStruct((sp, heads, seg), F32),
        ),
        in_specs=vmem_specs(3),
        out_specs=tuple(vmem_specs(3)),
        scratch_shapes=[dma((3, sp)), dma((3, sp))],
        compiler_params=params(0),
        name="exchange",
    )(key_vectors, value_vectors, cum_gate.T)

    partial = pl.pallas_call(
        functools.partial(attend_kernel, heads),
        out_shape=jax.ShapeDtypeStruct((seg, D), BF16),
        in_specs=vmem_specs(5),
        out_specs=vmem_specs(1)[0],
        scratch_shapes=[pltpu.VMEM((seg, width), BF16)],
        compiler_params=params(),
        name="attend",
    )(query_vectors, kall, vall, gall, out_weight)

    stream, rows, combs = pl.pallas_call(
        functools.partial(dispatch_kernel, sp, zn),
        out_shape=(
            jax.ShapeDtypeStruct((T, D), BF16),
            jax.ShapeDtypeStruct((sp, 2, zn, cap, D), BF16),
            jax.ShapeDtypeStruct((zn, 2 * T, slots), BF16),
        ),
        in_specs=vmem_specs(5),
        out_specs=tuple(vmem_specs(3)),
        scratch_shapes=[
            pltpu.VMEM((zn, T, D), BF16),
            pltpu.VMEM((zn, T, D), BF16),
            pltpu.VMEM((zn, T, D), BF16),
            pltpu.VMEM((zn, T, D), BF16),
            pltpu.VMEM((zn, slots, T), BF16),
            pltpu.VMEM((zn, sp, cap, D), BF16),
            dma((zn,)), dma((zn,)),
            dma((2, zn)), dma((2, zn)),
            dma((zn,)), dma((zn,)),
            dma((zn,)), dma((zn,)),
            dma((zn, sp)), dma((zn, sp)),
            dma((zn, sp)), dma((zn, sp)),
        ],
        compiler_params=params(1),
        name="dispatch",
    )(partial, tokens, norm_gain[None, :], place, comb)

    flat_rows = rows.reshape(-1, D)
    gate_value = jnp.dot(flat_rows, gate_weight[0], preferred_element_type=F32)
    up_value = jnp.dot(flat_rows, up_weight[0], preferred_element_type=F32)
    hidden = (jax.nn.silu(gate_value) * up_value).astype(BF16)
    y = jnp.dot(hidden, down_weight[0], preferred_element_type=F32).astype(BF16)

    return pl.pallas_call(
        functools.partial(combine_kernel, sp, zn),
        out_shape=jax.ShapeDtypeStruct((T, D), BF16),
        in_specs=vmem_specs(3),
        out_specs=vmem_specs(1)[0],
        scratch_shapes=[
            pltpu.VMEM((zn, sp, cap, D), BF16),
            pltpu.VMEM((zn, sp, cap, D), BF16),
            pltpu.VMEM((zn, sp, cap, D), BF16),
            pltpu.VMEM((zn, T, D), BF16),
            pltpu.VMEM((zn, T, D), BF16),
            dma((zn, sp)), dma((zn, sp)),
            dma((zn, sp)), dma((zn, sp)),
            dma((zn,)), dma((zn,)),
        ],
        compiler_params=params(2),
        name="combine",
    )(y.reshape(rows.shape), combs, stream)


def solution(mesh):
    in_specs = (
        P(("sp", "tp"), None),
        P("sp", "tp"),
        P("sp", "tp"),
        P("sp", "tp"),
        P("sp", "tp"),
        P("tp", None),
        P(),
        P("sp", None, "tp"),
        P("sp", None, "tp"),
        P("sp", "tp", None),
        P(("sp", "tp"), None),
        P(("sp", "tp"), None),
    )
    out_specs = P(("sp", "tp"), None)
    return jax.shard_map(shards, mesh=mesh, in_specs=in_specs, out_specs=out_specs, check_vma=False)
```

time: 363 us -> 221 us (0.61)
  waiting for transfers between devices: 255 us -> 0 us
  Pallas kernels: 0 us -> 185 us
  blocking collectives: 25.1 us -> 0 us
  between operations: 13.4 us -> 0.09 us
  matrix products: 42.6 us -> 30.5 us
  starting transfers between devices: 8.43 us -> 0 us
  local copies, waits for them, and re-layouts: 10.3 us -> 3.51 us
  other arithmetic: 6.2 us -> 2.24 us
    pallas_call x0 -> x4, Pallas kernels: none -> 185 us  [the longest x1 92.4 us: shards(): pl.pallas_call(functools.partial(dispatch_kernel, sp, zn), out_shape=(jax...]
    all_gather x4 -> x0, waiting for transfers between devices: 160 us -> none  [the longest x1 61.7 us: shards(): rows_in = lax.all_gather(row_block, 'tp', axis=0, tiled=True)]
    reduce_scatter x1 -> x0, waiting for transfers between devices: 68.5 us -> none  [shards(): lax.psum_scatter(jnp.dot(hidden, down_weight[0], preferred_element_type=j...]
    all_to_all x2 -> x0, waiting for transfers between devices: 24.1 us -> none  [the longest x1 15.4 us: shards(): lax.all_to_all(attended, 'tp', split_axis=0, concat_axis=1, tiled=True)]
    all_to_all x1 -> x0, blocking collectives: 15.3 us -> none  [shards(): lax.all_to_all(dispatch, 'sp', split_axis=0, concat_axis=0, tiled=True)]
    dot_general x6 -> x3, matrix products: 42.6 us -> 30.5 us  [the longest x1 20 us: shards(): y = jnp.dot(hidden, down_weight[0], preferred_element_type=F32).astype(BF16)]
    all_gather x1 -> x0, blocking collectives: 9.82 us -> none  [shards(): gate_rows = lax.all_gather(cum_gate, 'sp', axis=0, tiled=True)]
    all_to_all x2 -> x0, starting transfers between devices: 8.27 us -> none  [the longest x1 4.62 us: shards(): lax.all_to_all(attended, 'tp', split_axis=0, concat_axis=1, tiled=True)]
  transfers between devices with their start and end apart: 7 -> 0, of which waited for: 7 -> 0; matrix products, arithmetic and copies ran while one was open for 5% -> 0% of each run, Pallas kernels for 0% -> 0%
where the time goes in v1:
time: 221 us
  Pallas kernels  185 us (84%)
  matrix products  30.5 us (14%)
  local copies, waits for them, and re-layouts  3.51 us (2%)
  other arithmetic  2.24 us (1%)
    pallas_call x1, Pallas kernels, shards(): pl.pallas_call(functools.partial(dispatch_kernel, sp, zn), out_shape=(jax...  92.4 us
    pallas_call x1, Pallas kernels, shards(): pl.pallas_call(functools.partial(combine_kernel, sp, zn), out_shape=jax.S...  54.3 us
    pallas_call x1, Pallas kernels, shards(): pl.pallas_call(functools.partial(exchange_kernel, sp), out_shape=(jax.Sha...  29.7 us
    dot_general x1, matrix products, shards(): y = jnp.dot(hidden, down_weight[0], preferred_element_type=F32).astype(BF16)  20 us
    dot_general x1, matrix products, shards(): gate_value = jnp.dot(flat_rows, gate_weight[0], preferred_element_type=F32)  10.2 us
    pallas_call x1, Pallas kernels, shards(): pl.pallas_call(functools.partial(attend_kernel, heads), out_shape=jax.Sha...  8.18 us

profile of v1, /device:TPU:0, one launch (start us, length us, event | category | flops | bytes accessed | tf_op | source)
XLA Modules:
  0.0 220.9 jit_solution(15216553145426991812)
XLA Ops:
  0.0 0.8 copy.26
  0.8 0.1 eq.28
  0.9 0.2 fusion.7
  1.1 0.1 convert_element_type.24
  1.3 0.1 copy.27
  1.4 0.7 multiply_add_fusion
  2.1 0.1 fusion.8
  2.2 0.7 copy.28
  2.9 0.8 select_reduce_fusion
  3.7 0.0 copy-start
  3.7 0.6 pad_maximum_fusion.comb
  4.4 29.7 %exchange.1 = (bf16[4,512,256]{2,1,0:T(8,128)(2,1)}, bf16[4,512,256]{2,1,0:T(8,128)(2,1)}, f32[4,4,512]{2,1,0:T(4,128)}) custom-call(bf16[512,256]{1,0:T(8,128)(2,1)} %k.1, bf16[512,256]{1,0:T(8,128)(2,1)} %v.1, f32[4,512]{1,0:T(4,128)} %bitcast.20), custom_call_target="tpu_custom_call" | custom-call | tf_op jit(solution)/shard_map/exchange/pallas_call | solution.py:343
  34.0 8.2 %attend.1.p = bf16[512,2048]{1,0:T(8,128)(2,1)} custom-call(bf16[512,256]{1,0:T(8,128)(2,1)} %q.1, bf16[4,512,256]{2,1,0:T(8,128)(2,1)} %get-tuple-element.11.ka, bf16[4,512,256]{2,1,0:T(8,128)(2,1)} %get-tuple-element.12.va, f32[4,4,512]{2,1,0:T(4,128)} %get-tuple-element.13.ga, bf16[256,2048]{1,0:T(8,128)(2,1)} %w.1), custom_call_target="tpu_custom_call" | custom-call | tf_op jit(solution)/shard_map/attend/pallas_call | solution.py:357
  42.2 92.4 %dispatch.1 = (bf16[64,2048]{1,0:T(8,128)(2,1)}, bf16[4,2,4,48,2048]{4,3,2,1,0:T(8,128)(2,1)}, bf16[4,128,192]{2,1,0:T(8,128)(2,1)}) custom-call(bf16[512,2048]{1,0:T(8,128)(2,1)} %attend.1.p, bf16[64,2048]{1,0:T(8,128)(2,1)} %tok.1, f32[1,2048]{1,0:T(1,128)} %bitcast.21, bf16[192,64]{1,0:T(8,128)(2,1)} %bitcast.19, bf16[128,192]{1,0:T(8,128)(2,1)} %pad_maximum_fusion.comb), custom_call_target="tpu_custom_call" | custom-call | tf_op jit(solution)/shard_map/dispatch/pallas_call | solution.py:367
  134.6 0.0 copy-done
  134.6 10.2 %fusion.4 = f32[1536,896]{1,0:T(8,128)} fusion(bf16[1536,2048]{1,0:T(8,128)(2,1)} %bitcast.22, bf16[1,2048,896]{2,1,0:T(8,128)(2,1)S(1)} %copy-done), kind=kOutput, calls=%fused_computation.4 | convolution fusion | flops 5637144576 | bytes 15466496 | tf_op jit(solution)/shard_map/dot_general | solution.py:395
  144.8 20.0 %convolution_convert_fusion = bf16[1536,2048]{1,0:T(8,128)(2,1)} fusion(bf16[1,896,2048]{2,1,0:T(8,128)(2,1)} %param.21, f32[1536,896]{1,0:T(8,128)} %fusion.4, bf16[1536,2048]{1,0:T(8,128)(2,1)} %bitcast.23, bf16[1,2048,896]{2,1,0:T(8,128)(2,1)} %param.20), kind=kOutput, calls=%fused_computation | convolution fusion | flops 11285692416 | bytes 25427968 | tf_op jit(solution)/shard_map/dot_general | solution.py:398
  164.9 54.3 %combine.1 = bf16[64,2048]{1,0:T(8,128)(2,1)} custom-call(bf16[4,2,4,48,2048]{4,3,2,1,0:T(8,128)(2,1)} %bitcast.18, bf16[4,128,192]{2,1,0:T(8,128)(2,1)} %get-tuple-element.15.combs, bf16[64,2048]{1,0:T(8,128)(2,1)} %get-tuple-element.16.stream), custom_call_target="tpu_custom_call" | custom-call | tf_op jit(solution)/shard_map/combine/pallas_call | solution.py:400
  219.2 1.7 copy.30
  (4 shorter events, 0.0 us)
Async XLA Ops:
  3.7 130.9 %copy-start = (bf16[1,2048,896]{2,1,0:T(8,128)(2,1)S(1)}, bf16[1,2048,896]{2,1,0:T(8,128)(2,1)}, u32[]{:S(2)}) copy-start(bf16[1,2048,896]{2,1,0:T(8,128)(2,1)} %param.19) | copy-start | bytes 11010052

commit v2 on v1

v2 whole, which is shorter than its diff:
```python
import functools
import math

import jax
import jax.numpy as jnp
from jax import lax
from jax.experimental import pallas as pl
from jax.experimental.pallas import tpu as pltpu
from jax.sharding import PartitionSpec as P

MESH = pl.DeviceIdType.MESH
VMEM_LIMIT = 60 * 1024 * 1024
F32 = jnp.float32
BF16 = jnp.bfloat16


def rcopy(src, dst, ssem, rsem, where):
    return pltpu.make_async_remote_copy(
        src_ref=src, dst_ref=dst, send_sem=ssem, recv_sem=rsem, device_id=where, device_id_type=MESH
    )


def vmem_specs(count):
    return [pl.BlockSpec(memory_space=pltpu.VMEM)] * count


def attend_kernel(sp, heads, q, k, v, g, w, out, ka, va, ga, att, top_s, sum_s, acc_s, ssem, rsem):
    s = lax.axis_index("sp")
    barrier = pltpu.get_barrier_semaphore()
    for d in range(1, sp):
        pl.semaphore_signal(barrier, inc=1, device_id={"sp": lax.rem(s + d, sp)}, device_id_type=MESH)
    pl.semaphore_wait(barrier, sp - 1)
    pairs = ((k, ka), (v, va), (g, ga))

    def copy(n, d):
        src, dst = pairs[n]
        return rcopy(src, dst.at[d], ssem.at[n, d], rsem.at[n, d], {"sp": lax.rem(s + d, sp)})

    for d in range(1, sp):

        @pl.when(s + d < sp)
        def _():
            for n in range(3):
                copy(n, d).start()

    rows, width = q.shape
    hd = width // heads
    tile = math.gcd(rows, 256)
    log2e = 1.4426950408889634
    coef = hd ** (-0.5) * log2e
    units = [(h, i) for h in range(heads) for i in range(rows // tile)]

    def scores(h, i, kb, gb):
        qt = q[i * tile : (i + 1) * tile, h * hd : (h + 1) * hd]
        return (
            lax.dot_general(qt, kb, (((1,), (1,)), ((), ())), preferred_element_type=F32) * coef
            - gb * log2e
        )

    for h, i in units:
        cols = slice(h * hd, (h + 1) * hd)
        seen = (i + 1) * tile
        sc = scores(h, i, k[0:seen, cols], g[h : h + 1, 0:seen])
        row = lax.broadcasted_iota(jnp.int32, sc.shape, 0) + i * tile
        col = lax.broadcasted_iota(jnp.int32, sc.shape, 1)
        sc = jnp.where(col <= row, sc, -1e30)
        peak = jnp.max(sc, axis=1, keepdims=True)
        ex = jnp.exp2(sc - peak)
        at = slice(i * tile, seen)
        top_s[h, at] = peak
        sum_s[h, at] = jnp.sum(ex, axis=1, keepdims=True)
        acc_s[h, at] = jnp.dot(ex.astype(BF16), v[0:seen, cols], preferred_element_type=F32)

    def step(d, _):
        for n in range(3):
            copy(n, d).wait_recv()
        for h, i in units:
            cols = slice(h * hd, (h + 1) * hd)
            at = slice(i * tile, (i + 1) * tile)
            sc = scores(h, i, ka[d, :, cols], ga[d, h : h + 1, :])
            peak = top_s[h, at]
            new = jnp.maximum(peak, jnp.max(sc, axis=1, keepdims=True))
            ex = jnp.exp2(sc - new)
            fix = jnp.exp2(peak - new)
            top_s[h, at] = new
            sum_s[h, at] = sum_s[h, at] * fix + jnp.sum(ex, axis=1, keepdims=True)
            acc_s[h, at] = acc_s[h, at] * fix + jnp.dot(
                ex.astype(BF16), va[d, :, cols], preferred_element_type=F32
            )
        return 0

    lax.fori_loop(1, s + 1, step, 0)
    for h, i in units:
        at = slice(i * tile, (i + 1) * tile)
        att[at, h * hd : (h + 1) * hd] = (acc_s[h, at] / sum_s[h, at]).astype(BF16)
    wide = w.shape[1]
    chunk = math.gcd(wide, 512)
    for n in range(wide // chunk):
        cut = slice(n * chunk, (n + 1) * chunk)
        out[:, cut] = jnp.dot(att[...], w[:, cut], preferred_element_type=F32).astype(BF16)
    for d in range(1, sp):

        @pl.when(s + d < sp)
        def _():
            for n in range(3):
                copy(n, d).wait_send()


def greet(sp, zn, s, z, c, partner):
    barrier = pltpu.get_barrier_semaphore()
    pl.semaphore_signal(barrier, inc=1, device_id={"tp": partner}, device_id_type=MESH)
    for i in range(1, zn):
        pl.semaphore_signal(
            barrier, inc=1, device_id={"tp": 2 * lax.rem(z + i, zn) + c}, device_id_type=MESH
        )
    for d in range(1, sp):
        pl.semaphore_signal(barrier, inc=1, device_id={"sp": lax.rem(s + d, sp)}, device_id_type=MESH)
    pl.semaphore_wait(barrier, 1 + (zn - 1) + (sp - 1))


def experts_kernel(
    sp, zn, p, tok, gain, place, comb, wg_in, wu_in, wd_in, out,
    wg, wu, wd, xr, cb, zr, ng, pg, combs, db, rows, hid, y, pr, cs, eb, mb, rr, keep,
    ws, xs, xrs, as_, ars, zs, zrs, ns, nrs, ds_, drs, fs, frs, ps, prs, es, ers, ms, mrs,
):
    s, t = lax.axis_index("sp"), lax.axis_index("tp")
    z, c = t // 2, lax.rem(t, 2)
    partner = t + 1 - 2 * c
    T, D = tok.shape
    cap = rows.shape[3]
    loads = [
        pltpu.make_async_copy(a.at[0], b, ws.at[n])
        for n, (a, b) in enumerate(((wg_in, wg), (wu_in, wu), (wd_in, wd)))
    ]
    for load in loads:
        load.start()
    greet(sp, zn, s, z, c, partner)
    offs = [0] + sorted(range(1, zn), key=lambda i: -min(i, zn - i))
    outs = offs[1:] + [0]

    def at_z(i):
        return 2 * lax.rem(z + i, zn) + c

    def peer(d):
        return lax.rem(s + d, sp)

    def behind(d):
        return lax.rem(s + sp - d, sp)

    def swap(i):
        zz = lax.rem(z + outs[i], zn)
        src = p.at[pl.ds(pl.multiple_of((2 * zz + 1 - c) * T, 16), T)]
        return rcopy(src, xr.at[i], xs.at[i], xrs.at[i], {"tp": partner})

    def aux(n, i):
        src, dst = ((place, pg), (comb, combs))[n]
        return rcopy(src, dst.at[i], as_.at[n, i], ars.at[n, i], {"tp": at_z(offs[i])})

    def reduce_to(i):
        return rcopy(cb.at[i], zr.at[i], zs.at[i], zrs.at[i], {"tp": at_z(outs[i])})

    def spread(i):
        return rcopy(ng.at[0], ng.at[i], ns.at[i], nrs.at[i], {"tp": at_z(offs[i])})

    def route(i, d):
        return rcopy(
            db.at[i, peer(d)], rows.at[i, s, c], ds_.at[i, d], drs.at[i, d], {"sp": peer(d)}
        )

    def routed(i, d):
        return rcopy(
            db.at[i, peer(d)], rows.at[i, behind(d), c], ds_.at[i, d], drs.at[i, d], {"sp": peer(d)}
        )

    def forward(i, d):
        ref = rows.at[i, behind(d), c]
        return rcopy(ref, ref, fs.at[i, d], frs.at[i, d], {"tp": partner})

    def forwarded(i, d):
        ref = rows.at[i, behind(d), 1 - c]
        return rcopy(ref, ref, fs.at[i, d], frs.at[i, d], {"tp": partner})

    def swap_out(i, d):
        return rcopy(y.at[i, peer(d), 1 - c], pr.at[i, d], ps.at[i, d], prs.at[i, d], {"tp": partner})

    def back(i, d, slot):
        return rcopy(cs.at[i, d], eb.at[i, slot], es.at[i, d], ers.at[i, d], {"sp": peer(d)})

    def reduce_out(i):
        return rcopy(
            mb.at[i], rr.at[i], ms.at[i], mrs.at[i], {"tp": at_z(zn - offs[i])}
        )

    def dispatch(i):
        if i > 0:
            aux(0, i).wait_recv()
            spread(i).wait_recv()
        moved = jnp.dot(pg[i], ng[i], preferred_element_type=F32)
        for e in range(sp):
            db[i, e] = moved[e * cap : (e + 1) * cap].astype(BF16)
        for d in range(1, sp):
            route(i, d).start()
        rows[i, s, c] = db[i, s]
        forward(i, 0).start()

    def pass_on(i):
        def arrive(d, _):
            routed(i, d).wait_recv()
            forward(i, d).start()
            return 0

        lax.fori_loop(1, sp, arrive, 0)

    def each(count, body):
        if count * rows.shape[1] <= 64:
            for n in range(count):
                body(n)
        else:
            lax.fori_loop(0, count, lambda n, _: (body(n), 0)[1], 0)

    def expert(i):
        def landed(d, _):
            forwarded(i, d).wait_recv()
            return 0

        lax.fori_loop(0, sp, landed, 0)
        x = rows.at[i]
        many = sp * 2 * cap
        units = wg.shape[1]
        step = 256

        def into(start, size):
            cut = pl.ds(start, size)
            xv = x[...].reshape(many, D)
            gate = jnp.dot(xv, wg[:, cut], preferred_element_type=F32)
            up = jnp.dot(xv, wu[:, cut], preferred_element_type=F32)
            hid[:, cut] = (gate / (1.0 + jnp.exp(-gate)) * up).astype(BF16)

        each(units // step, lambda n: into(pl.multiple_of(n * step, step), step))
        if units % step:
            into(units - units % step, units % step)
        chunk = math.gcd(D, 512)

        def down(n):
            cut = pl.ds(pl.multiple_of(n * chunk, chunk), chunk)
            got = jnp.dot(hid[...], wd[:, cut], preferred_element_type=F32).astype(BF16)
            y[i, :, :, :, cut] = got.reshape(sp, 2, cap, chunk)

        each(D // chunk, down)
        for d in list(range(1, sp)) + [0]:
            swap_out(i, d).start()

    def give_back(i):
        def both(d):
            swap_out(i, d).wait_recv()
            return (y[i, peer(d), c].astype(F32) + pr[i, d].astype(F32)).astype(BF16)

        def send(d, _):
            cs[i, d] = both(d)
            back(i, d, s).start()
            return 0

        lax.fori_loop(1, sp, send, 0)
        eb[i, s] = both(0)

    def mix(i):
        if i > 0:
            aux(1, i).wait_recv()
        for d in range(1, sp):
            back(i, d, behind(d)).wait_recv()
        mixed = jnp.dot(combs[i], eb[i].reshape(sp * cap, D), preferred_element_type=F32)
        mixed = mixed[0:T] + mixed[T : 2 * T]
        if i > 0:
            mb[i] = mixed.astype(BF16)
            reduce_out(i).start()
        else:
            keep[...] = mixed

    for i in range(zn):
        swap(i).start()
    for i in range(1, zn):
        for n in range(2):
            aux(n, i).start()
    pg[0] = place[...]
    combs[0] = comb[...]
    own = None
    for i in range(zn):
        swap(i).wait_recv()
        zz = lax.rem(z + outs[i], zn)
        both = p[pl.ds(pl.multiple_of((2 * zz + c) * T, 16), T), :].astype(F32) + xr[i].astype(F32)
        if i < zn - 1:
            cb[i] = both.astype(BF16)
            reduce_to(i).start()
        else:
            own = both
    for i in range(zn - 1):
        reduce_to(i).wait_recv()
        own = own + zr[i].astype(F32)
    st = (tok[...].astype(F32) + own).astype(BF16)
    out[...] = st
    wide = st.astype(F32)
    inverse = lax.rsqrt(jnp.mean(wide * wide, axis=1, keepdims=True) + 1e-05)
    ng[0] = (wide * inverse * gain[...]).astype(BF16)
    for i in range(1, zn):
        spread(i).start()
    dispatch(0)
    if zn > 1:
        dispatch(1)
    for load in loads:
        load.wait()
    for i in range(zn):
        pass_on(i)
        if i + 2 < zn:
            dispatch(i + 2)
        expert(i)
        if i >= 1:
            give_back(i - 1)
        if i >= 2:
            mix(i - 2)
    give_back(zn - 1)
    if zn > 1:
        mix(zn - 2)
    mix(zn - 1)
    total = out[...].astype(F32) + keep[...]
    for i in range(1, zn):
        reduce_out(i).wait_recv()
        total = total + rr[i].astype(F32)
    out[...] = total.astype(BF16)
    for i in range(zn):
        swap(i).wait_send()
        if i < zn - 1:
            reduce_to(i).wait_send()
        if i > 0:
            spread(i).wait_send()
            reduce_out(i).wait_send()
            for n in range(2):
                aux(n, i).wait_send()

        def drain(d, _):
            forward(i, d).wait_send()
            swap_out(i, d).wait_send()
            return 0

        lax.fori_loop(0, sp, drain, 0)
        for d in range(1, sp):
            route(i, d).wait_send()
            back(i, d, s).wait_send()


def params(cid=None):
    if cid is None:
        return pltpu.CompilerParams(vmem_limit_bytes=VMEM_LIMIT)
    return pltpu.CompilerParams(
        collective_id=cid, has_side_effects=True, vmem_limit_bytes=VMEM_LIMIT
    )


def shards(
    tokens,
    query_vectors,
    key_vectors,
    value_vectors,
    cum_gate,
    out_weight,
    norm_gain,
    gate_weight,
    up_weight,
    down_weight,
    expert_ids,
    route_weights,
):
    sp = lax.axis_size("sp")
    tp = lax.axis_size("tp")
    zn = tp // 2
    seg, width = query_vectors.shape
    heads = cum_gate.shape[1]
    T, D = tokens.shape
    dma = pltpu.SemaphoreType.DMA

    n_experts = gate_weight.shape[0] * sp
    top = expert_ids.shape[1]
    cap = max(2, 3 * T * top // (2 * n_experts))
    cap = -(-cap // 8) * 8
    slots = n_experts * cap
    flat = expert_ids.reshape(-1)
    hits = (flat[:, None] == jnp.arange(n_experts, dtype=jnp.int32)[None, :]).astype(F32)
    lower = jnp.tril(jnp.ones((flat.shape[0], flat.shape[0]), F32), -1)
    earlier = jnp.dot(lower, hits, preferred_element_type=F32)
    slot = (flat * cap + jnp.sum(earlier * hits, axis=1).astype(jnp.int32)).reshape(T, top)
    match = slot[:, :, None] == jnp.arange(slots, dtype=jnp.int32)[None, None, :]
    place = jnp.any(match, axis=1).astype(BF16).T
    weight = jnp.sum(jnp.where(match, route_weights[:, :, None], 0.0), axis=1)
    high = lax.reduce_precision(weight, 8, 7)
    comb = jnp.concatenate([high, weight - high], axis=0).astype(BF16)

    fh = gate_weight.shape[2]
    partial = pl.pallas_call(
        functools.partial(attend_kernel, sp, heads),
        out_shape=jax.ShapeDtypeStruct((seg, D), BF16),
        in_specs=vmem_specs(5),
        out_specs=vmem_specs(1)[0],
        scratch_shapes=[
            pltpu.VMEM((sp, seg, width), BF16),
            pltpu.VMEM((sp, seg, width), BF16),
            pltpu.VMEM((sp, heads, seg), F32),
            pltpu.VMEM((seg, width), BF16),
            pltpu.VMEM((heads, seg, 1), F32),
            pltpu.VMEM((heads, seg, 1), F32),
            pltpu.VMEM((heads, seg, width // heads), F32),
            dma((3, sp)), dma((3, sp)),
        ],
        compiler_params=params(0),
        name="attend",
    )(query_vectors, key_vectors, value_vectors, cum_gate.T, out_weight)

    def vm(*shape, kind=BF16):
        return pltpu.VMEM(shape, kind)

    return pl.pallas_call(
        functools.partial(experts_kernel, sp, zn),
        out_shape=jax.ShapeDtypeStruct((T, D), BF16),
        in_specs=vmem_specs(5) + [pl.BlockSpec(memory_space=pl.ANY)] * 3,
        out_specs=vmem_specs(1)[0],
        scratch_shapes=[
            vm(D, fh), vm(D, fh), vm(fh, D),
            vm(zn, T, D), vm(zn, T, D), vm(zn, T, D), vm(zn, T, D),
            vm(zn, slots, T), vm(zn, 2 * T, slots),
            vm(zn, sp, cap, D),
            vm(zn, sp, 2, cap, D),
            vm(sp * 2 * cap, fh),
            vm(zn, sp, 2, cap, D),
            vm(zn, sp, cap, D), vm(zn, sp, cap, D), vm(zn, sp, cap, D),
            vm(zn, T, D), vm(zn, T, D),
            vm(T, D, kind=F32),
            dma((3,)),
            dma((zn,)), dma((zn,)),
            dma((2, zn)), dma((2, zn)),
            dma((zn,)), dma((zn,)),
            dma((zn,)), dma((zn,)),
            dma((zn, sp)), dma((zn, sp)),
            dma((zn, sp)), dma((zn, sp)),
            dma((zn, sp)), dma((zn, sp)),
            dma((zn, sp)), dma((zn, sp)),
            dma((zn,)), dma((zn,)),
        ],
        compiler_params=params(1),
        name="experts",
    )(partial, tokens, norm_gain[None, :], place, comb, gate_weight, up_weight, down_weight)


def solution(mesh):
    in_specs = (
        P(("sp", "tp"), None),
        P("sp", "tp"),
        P("sp", "tp"),
        P("sp", "tp"),
        P("sp", "tp"),
        P("tp", None),
        P(),
        P("sp", None, "tp"),
        P("sp", None, "tp"),
        P("sp", "tp", None),
        P(("sp", "tp"), None),
        P(("sp", "tp"), None),
    )
    out_specs = P(("sp", "tp"), None)
    return jax.shard_map(shards, mesh=mesh, in_specs=in_specs, out_specs=out_specs, check_vma=False)
```

time: 221 us -> 174 us (0.79)
  matrix products: 30.5 us -> 0.22 us
  Pallas kernels: 185 us -> 168 us
    dot_general x2 -> x0, matrix products: 30.3 us -> none  [the longest x1 20 us: shards(): y = jnp.dot(hidden, down_weight[0], preferred_element_type=F32).astype(BF16)]
    pallas_call x4 -> x2, Pallas kernels: 185 us -> 168 us  [the longest x1 138 us: shards(): pl.pallas_call(functools.partial(experts_kernel, sp, zn), out_shape=jax.S...]
where the time goes in v2:
time: 174 us
  Pallas kernels  168 us (97%)
  local copies, waits for them, and re-layouts  3.5 us (2%)
  other arithmetic  2.24 us (1%)
    pallas_call x1, Pallas kernels, shards(): pl.pallas_call(functools.partial(experts_kernel, sp, zn), out_shape=jax.S...  138 us
    pallas_call x1, Pallas kernels, shards(): pl.pallas_call(functools.partial(attend_kernel, sp, heads), out_shape=jax...  29.8 us

profile of v2, /device:TPU:0, one launch (start us, length us, event | category | flops | bytes accessed | tf_op | source)
XLA Modules:
  0.0 173.8 jit_solution(16542616564450663522)
XLA Ops:
  0.0 0.8 copy.26
  0.8 0.1 eq.28
  0.9 0.2 fusion
  1.1 0.1 convert_element_type.18
  1.3 0.1 copy.27
  1.4 0.7 multiply_add_fusion
  2.1 0.1 fusion.1
  2.2 0.7 copy.28
  2.9 0.8 select_reduce_fusion
  3.7 0.6 pad_maximum_fusion.comb
  4.3 29.8 %attend.1.p = bf16[512,2048]{1,0:T(8,128)(2,1)} custom-call(bf16[512,256]{1,0:T(8,128)(2,1)} %q.1, bf16[512,256]{1,0:T(8,128)(2,1)} %k.1, bf16[512,256]{1,0:T(8,128)(2,1)} %v.1, f32[4,512]{1,0:T(4,128)} %bitcast.4, bf16[256,2048]{1,0:T(8,128)(2,1)} %w.1), custom_call_target="tpu_custom_call" | custom-call | tf_op jit(solution)/shard_map/attend/pallas_call | solution.py:397
  34.1 138.0 %experts.1 = bf16[64,2048]{1,0:T(8,128)(2,1)} custom-call(bf16[512,2048]{1,0:T(8,128)(2,1)} %attend.1.p, bf16[64,2048]{1,0:T(8,128)(2,1)} %tok.1, f32[1,2048]{1,0:T(1,128)} %bitcast.5, bf16[192,64]{1,0:T(8,128)(2,1)} %bitcast.3, bf16[128,192]{1,0:T(8,128)(2,1)} %pad_maximum_fusion.comb, bf16[1,2048,896]{2,1,0:T(8,128)(2,1)} %wg_in.1, ...), custom_call_target="tpu_custom_call" | custom-call | tf_op jit(solution)/shard_map/experts/pallas_call | solution.py:419
  172.1 1.7 copy.30
  (4 shorter events, 0.0 us)
